TPU v7x, 32 devices: a whole 2x2x4 slice. The times are simulated.
32 devices in a mesh: sp: 8 (over z, x), tp: 4 (over y, core).
Axes of the slice: x: 2, y: 2, z: 4, core: 2. Of those that a mesh axis runs over, the one named last changes fastest.
Arguments:
- resid: bfloat16 [2048, 2048], P('sp'), may hold values from -6 to 6
- query_one: bfloat16 [2048, 1024], P('sp', 'tp'), may hold values from -400 to 400
- query_two: bfloat16 [2048, 1024], P('sp', 'tp'), may hold values from -400 to 400
- key_one: bfloat16 [2048, 1024], P('sp', 'tp'), may hold values from -8 to 8
- key_two: bfloat16 [2048, 1024], P('sp', 'tp'), may hold values from -8 to 8
- values: bfloat16 [2048, 2048], P('sp', 'tp'), may hold values from -6 to 6
- documents: int32 [2048], P('sp'), may hold values from 0 to 1, never falling along the last dimension, each value on 1 to 1280 neighbouring positions
- mix_lambda: float32 [16], P('tp'), may hold values from 0.3 to 0.8
- head_gain: float32 [128], replicated, may hold values from 0.1 to 1.9
- out_weight: bfloat16 [2048, 2048], P('tp'), may hold values from -0.125 to 0.125
- ffn_gain: float32 [2048], replicated, may hold values from 0.1 to 1.9
- routes: int32 [2048, 4], P('sp'), may hold values from 0 to 31, all different within a row; in each aligned block of 256 rows (0 to 255, 256 to 511, ...) at most 64 rows name the same one
- route_weight: float32 [2048, 4], P('sp'), may hold values from 0.2 to 0.9
- expert_gate: bfloat16 [32, 2048, 512], P(('sp', 'tp')), may hold values from -0.125 to 0.125
- expert_up: bfloat16 [32, 2048, 512], P(('sp', 'tp')), may hold values from -0.125 to 0.125
- expert_down: bfloat16 [32, 512, 2048], P(('sp', 'tp')), may hold values from -0.25 to 0.25
- shared_gate: bfloat16 [2048, 512], P(None, 'tp'), may hold values from -0.125 to 0.125
- shared_up: bfloat16 [2048, 512], P(None, 'tp'), may hold values from -0.125 to 0.125
- shared_down: bfloat16 [512, 2048], P('tp'), may hold values from -0.25 to 0.25
Outputs:
- layer_out: bfloat16 [2048, 2048], P(('sp', 'tp'))
Inputs may be any that keep to these rules, and one draw needn't show every extreme that they name: `documents`: document numbers never fall along the positions; each document has 1 to 1280 positions and one has exactly 1280. `routes`: A row names 4 different experts. In each aligned block of 256 rows no expert is named by more than 64 rows, a bound that some block reaches.
All inputs are finite; a program needn't handle non-finite values.
Results may differ from a plain program's by a relative error of at most 0.018.
Values may be sent and summed in bfloat16 or wider, within the bound.
A program may use at most 128 MiB of HBM per device.

v0:
```python
import jax
import jax.numpy as jnp
from jax import lax
from jax.sharding import PartitionSpec as P

NEG_FILL = -1e30
HEAD_SCALE = 0.8


def rms_scale(values_in, eps_value):
    return lax.rsqrt(jnp.mean(values_in * values_in, axis=-1, keepdims=True) + eps_value)


def local(
    resid,
    query_one,
    query_two,
    key_one,
    key_two,
    values,
    documents,
    mix_lambda,
    head_gain,
    out_weight,
    ffn_gain,
    routes,
    route_weight,
    expert_gate,
    expert_up,
    expert_down,
    shared_gate,
    shared_up,
    shared_down,
):
    tok_rows = query_one.shape[0]
    head_count = mix_lambda.shape[0]
    head_width = query_one.shape[1] // head_count
    value_width = values.shape[1] // head_count
    model_width = resid.shape[1]
    score_scale = head_width ** (-0.5)
    seq_size = lax.axis_size("sp")
    tp_size = lax.axis_size("tp")
    query_pos = lax.axis_index("sp") * tok_rows + jnp.arange(tok_rows, dtype=jnp.int32)
    query_first = query_one.reshape(tok_rows, head_count, head_width)
    query_second = query_two.reshape(tok_rows, head_count, head_width)
    lambda_col = mix_lambda[:, None, None]
    first_doc = documents[0]
    last_pos = query_pos[tok_rows - 1]

    def masks(key_docs):
        key_pos = jnp.arange(key_docs.shape[0], dtype=jnp.int32)
        return (
            (key_pos[None, :] <= query_pos[:, None]) & (key_docs[None, :] == documents[:, None])
        )[None]

    def needed(key_docs, offset):
        return (offset <= last_pos) & (jnp.max(key_docs) >= first_doc)

    def scores(query_block, key_block):
        keyed = key_block.reshape(key_block.shape[0], head_count, head_width)
        return (
            jnp.einsum("qhd,khd->hqk", query_block, keyed, preferred_element_type=jnp.float32)
            * score_scale
        )

    empty_max = jnp.full((head_count, tok_rows), NEG_FILL, jnp.float32)
    empty_sum = jnp.zeros((head_count, tok_rows), jnp.float32)
    stats_init = ((empty_max, empty_sum), (empty_max, empty_sum))
    value_init = jnp.zeros((head_count, tok_rows, value_width), jnp.float32)
    key_first = lax.all_gather(key_one, "sp", axis=0, tiled=True)
    key_second = lax.all_gather(key_two, "sp", axis=0, tiled=True)
    key_docs = lax.all_gather(documents, "sp", axis=0, tiled=True)

    def stats_update(current):
        allowed = masks(key_docs)
        result = []
        for query_block, key_block, (top_now, sum_now) in (
            (query_first, key_first, current[0]),
            (query_second, key_second, current[1]),
        ):
            masked = jnp.where(allowed, scores(query_block, key_block), NEG_FILL)
            top_next = jnp.maximum(top_now, jnp.max(masked, axis=-1))
            fresh = jnp.where(allowed, jnp.exp(masked - top_next[:, :, None]), 0.0)
            result.append((top_next, jnp.sum(fresh, axis=-1)))
        return tuple(result)

    def stats_keep(current):
        return current

    soft_stats = lax.cond(needed(key_docs, jnp.int32(0)), stats_update, stats_keep, stats_init)
    apply_key_first = lax.all_gather(key_one, "sp", axis=0, tiled=True)
    apply_key_second = lax.all_gather(key_two, "sp", axis=0, tiled=True)
    value_block = lax.all_gather(values, "sp", axis=0, tiled=True)
    apply_key_docs = lax.all_gather(documents, "sp", axis=0, tiled=True)

    def apply_update(current):
        allowed = masks(apply_key_docs)
        probs = []
        for query_block, key_block, (top_all, sum_all) in (
            (query_first, apply_key_first, soft_stats[0]),
            (query_second, apply_key_second, soft_stats[1]),
        ):
            raw = scores(query_block, key_block)
            probs.append(
                jnp.where(allowed, jnp.exp(raw - top_all[:, :, None]), 0.0) / sum_all[:, :, None]
            )
        weights = (probs[0] - lambda_col * probs[1]).astype(jnp.bfloat16)
        valued = value_block.reshape(value_block.shape[0], head_count, value_width)
        return current + jnp.einsum(
            "hqk,khv->hqv", weights, valued, preferred_element_type=jnp.float32
        )

    def apply_keep(current):
        return current

    head_out = lax.cond(needed(apply_key_docs, jnp.int32(0)), apply_update, apply_keep, value_init)
    normed_heads = (head_out * rms_scale(head_out, 1e-05) * head_gain * HEAD_SCALE).astype(
        jnp.bfloat16
    )
    attn_rows = normed_heads.transpose(1, 0, 2).reshape(tok_rows, head_count * value_width)
    share_rows = tok_rows // tp_size
    own_start = lax.axis_index("tp") * share_rows
    proj_term = jnp.dot(attn_rows, out_weight, preferred_element_type=jnp.float32)
    projected = lax.psum(proj_term.astype(jnp.bfloat16), "tp").astype(jnp.float32)
    mixed_all = resid.astype(jnp.float32) + projected
    normed_all = (mixed_all * rms_scale(mixed_all, 1e-06) * ffn_gain).astype(jnp.bfloat16)
    mixed_own = lax.dynamic_slice_in_dim(mixed_all, own_start, share_rows, 0)
    route_slots = routes.shape[1]
    capacity = max(2, 2 * tok_rows * route_slots // (seq_size * tp_size))
    assign_total = tok_rows * route_slots
    flat_expert = routes.reshape(assign_total)
    flat_weight = route_weight.reshape(assign_total)
    assign_token = jnp.arange(assign_total, dtype=jnp.int32) // route_slots
    is_mine = flat_expert % tp_size == lax.axis_index("tp")
    target = flat_expert // tp_size
    one_hot = (
        (target[:, None] == jnp.arange(seq_size, dtype=jnp.int32)[None, :]) & is_mine[:, None]
    ).astype(jnp.int32)
    slot_rank = jnp.sum(jnp.cumsum(one_hot, axis=0) * one_hot, axis=1) - 1
    slot_id = jnp.where(is_mine, target * capacity + slot_rank, -1)
    slot_total = seq_size * capacity
    matches = slot_id[None, :] == jnp.arange(slot_total, dtype=jnp.int32)[:, None]
    slot_token = jnp.sum(jnp.where(matches, assign_token[None, :], 0), axis=1)
    slot_live = jnp.any(matches, axis=1)
    outgoing = jnp.where(
        slot_live[:, None], normed_all[slot_token], jnp.zeros((), jnp.bfloat16)
    ).reshape(seq_size, capacity, model_width)
    arrived = lax.all_to_all(outgoing, "sp", split_axis=0, concat_axis=0, tiled=True)
    item_count = arrived.shape[1]
    flat_rows = arrived.reshape(seq_size * item_count, model_width)
    gate_part = jnp.dot(flat_rows, expert_gate[0], preferred_element_type=jnp.float32)
    up_part = jnp.dot(flat_rows, expert_up[0], preferred_element_type=jnp.float32)
    hidden = (jax.nn.silu(gate_part) * up_part).astype(jnp.bfloat16)
    result = jnp.dot(hidden, expert_down[0], preferred_element_type=jnp.float32).astype(
        jnp.bfloat16
    )
    returned = lax.all_to_all(
        result.reshape(seq_size, item_count, model_width),
        "sp",
        split_axis=0,
        concat_axis=0,
        tiled=True,
    )
    returned_flat = returned.reshape(slot_total, model_width)
    picked = returned_flat[jnp.maximum(slot_id, 0)].astype(jnp.float32)
    picked_weight = jnp.where(is_mine, flat_weight, 0.0)
    routed = jnp.sum(
        (picked * picked_weight[:, None]).reshape(tok_rows, route_slots, model_width), axis=1
    )
    shared_act = (
        jax.nn.silu(jnp.dot(normed_all, shared_gate, preferred_element_type=jnp.float32))
        * jnp.dot(normed_all, shared_up, preferred_element_type=jnp.float32)
    ).astype(jnp.bfloat16)
    shared_out = jnp.dot(shared_act, shared_down, preferred_element_type=jnp.float32)
    ffn_own = lax.psum_scatter(
        (routed + shared_out).astype(jnp.bfloat16), "tp", scatter_dimension=0, tiled=True
    ).astype(jnp.float32)
    return (mixed_own + ffn_own).astype(jnp.bfloat16)


def solution(mesh):
    placed = (
        P("sp", None),
        P("sp", "tp"),
        P("sp", "tp"),
        P("sp", "tp"),
        P("sp", "tp"),
        P("sp", "tp"),
        P("sp"),
        P("tp"),
        P(),
        P("tp", None),
        P(),
        P("sp", None),
        P("sp", None),
        P(("sp", "tp"), None, None),
        P(("sp", "tp"), None, None),
        P(("sp", "tp"), None, None),
        P(None, "tp"),
        P(None, "tp"),
        P("tp", None),
    )
    return jax.shard_map(
        local, mesh=mesh, in_specs=placed, out_specs=P(("sp", "tp"), None), check_vma=False
    )
```

profile of v0, /device:TPU:0, one launch (start us, length us, event | category | flops | bytes accessed | tf_op | source)
XLA Modules:
  0.0 388.5 jit_solution(5894218725486632129)
XLA Ops:
  15.9 22.3 %all-gather = s32[8,1,256]{2,1,0:T(1,128)S(1)} all-gather(s32[1,1,256]{2,1,0:T(1,128)S(1)} %bitcast.92), channel_id=1, replica_groups=mesh['sp'=8,'tp'=4] {'sp'}, dimensions={0}, use_global_device_ids=true | all-gather | bytes 9216 | tf_op jit(solution)/shard_map/all_gather | solution.py:94
  42.9 8.6 %all-gather.5.cloned.1.call-done = bf16[2048,256]{0,1:T(8,128)(2,1)} async-done(((bf16[256,256]{0,1:T(8,128)(2,1)}), bf16[2048,256]{0,1:T(8,128)(2,1)}) %all-gather.5.cloned.1.call-update) | async-done | bytes 1048592 | tf_op jit(solution)/shard_map/all_gather | solution.py:91
  51.6 40.5 %all-gather.7.cloned.1.call-done = bf16[2048,256]{0,1:T(8,128)(2,1)} async-done(((bf16[256,256]{0,1:T(8,128)(2,1)}), bf16[2048,256]{0,1:T(8,128)(2,1)}) %all-gather.7.cloned.1.call-update) | async-done | bytes 1048592 | tf_op jit(solution)/shard_map/all_gather | solution.py:71
  92.0 12.4 %conditional.2 = (f32[4,256]{1,0:T(4,128)}, f32[4,256]{1,0:T(4,128)S(1)}, f32[4,256]{1,0:T(4,128)}, f32[4,256]{1,0:T(4,128)S(1)}) conditional(s32[]{:T(128)} %convert_element_type.53, () %tuple.24, (s32[256]{0:T(256)S(1)}, s32[2048]{0:T(1024)S(1)}, s32[256]{0:T(256)S(1)}, bf16[2048,256]{0,1:T(8,128)(2,1)}, bf16[256,4,64]{0,2,1:T(8,128)(2,1)S(1)}, ...), branch_computations={%region_1.0_spmd, %region_2.7_spmd} | conditional | flops 571996160 | bytes 50120764 | solution.py:90
  92.0 2.6 fusion.55
  95.2 3.1 fusion.1
  98.9 5.5 %select_reduce_fusion = (f32[4,256]{1,0:T(4,128)S(1)}, f32[4,256]{1,0:T(4,128)S(1)}) fusion(f32[4,256,2048]{2,1,0:T(8,128)S(1)} %get-tuple-element.106, f32[4,256]{1,0:T(4,128)} %get-tuple-element.122, pred[256,2048]{1,0:T(8,128)(4,1)S(1)} %fusion.2, f32[4,256]{1,0:T(4,128)} %get-tuple-element.120, f32[4,256,2048]{2,1,0:T(8,128)S(1)} %fusion.55), kind=kLoop, calls=%fused_computation.2 | loop fusion | flops 20969472 | bytes 17317888 | tf_op jit(solution)/shard_map/cond/branch_1_fun/reduce_sum | solution.py:84
  104.4 39.0 %all-gather.9.cloned.1.call-done = bf16[2048,512]{0,1:T(8,128)(2,1)} async-done(((bf16[256,512]{0,1:T(8,128)(2,1)}), bf16[2048,512]{0,1:T(8,128)(2,1)}) %all-gather.9.cloned.1.call-update) | async-done | bytes 2097168 | tf_op jit(solution)/shard_map/all_gather | solution.py:93
  143.5 16.7 %conditional.3 = (f32[4,256,128]{1,2,0:T(8,128)S(1)}, f32[4,256,1]{1,0,2:T(4,128)S(1)}) conditional(s32[]{:T(128)} %convert_element_type.53, () %tuple.23, (s32[256]{0:T(256)S(1)}, s32[2048]{0:T(1024)S(1)}, s32[256]{0:T(256)S(1)}, bf16[2048,256]{0,1:T(8,128)(2,1)}, bf16[256,4,64]{0,2,1:T(8,128)(2,1)S(1)}, /*index=5*/f32[4,256]{1,0:T(4,128)}, ...), branch_computations={%region_7.8_spmd, %region_8.0_spmd} | conditional | flops 1098644480 | bytes 22837280 | solution.py:116
  143.5 5.7 %fusion.56 = f32[4,256,2048]{2,1,0:T(8,128)} fusion(bf16[256,4,64]{0,2,1:T(8,128)(2,1)S(1)} %get-tuple-element.58, bf16[2048,4,64]{0,2,1:T(8,128)(2,1)} %bitcast.75), kind=kOutput, calls=%fused_computation.113 | convolution fusion | flops 268435456 | bytes 9568256 | tf_op jit(solution)/shard_map/cond/branch_1_fun/qhd,khd->hqk/dot_general | solution.py:62
  150.6 9.6 %multiply_reduce_fusion = (f32[4,256]{1,0:T(4,128)S(1)}, f32[4,256,128]{1,2,0:T(8,128)S(1)}) fusion(bf16[2048,4,128]{0,2,1:T(8,128)(2,1)} %bitcast.95, f32[4,256,2048]{2,1,0:T(8,128)} %fusion.56, bf16[256,4,64]{0,2,1:T(8,128)(2,1)S(1)} %get-tuple-element.63, bf16[2048,4,64]{0,2,1:T(8,128)(2,1)} %bitcast.82, f32[4,256]{1,0:T(4,128)S(1)} %get-tuple-element.66, ...), kind=kOutput, calls=%fused_computation.21 | convolution fusion | flops 828636160 | bytes 12734480 | tf_op jit(solution)/shard_map/cond/branch_1_fun/hqk,khv->hqv/dot_general | solution.py:109
  160.4 3.4 convolution_convert_fusion.1
  164.6 33.9 %all-reduce.2.cloned.1.call-done = bf16[256,2048]{1,0:T(8,128)(2,1)} async-done(((bf16[256,2048]{1,0:T(8,128)(2,1)}), bf16[256,2048]{1,0:T(8,128)(2,1)}) %all-reduce.2.cloned.1.call-update) | async-done | bytes 1048592 | tf_op jit(solution)/shard_map/psum | solution.py:124
  198.5 3.1 convert_add_fusion
  202.2 3.3 gather_fusion
  207.3 53.2 %all_to_all.10 = bf16[8,64,2048]{2,1,0:T(8,128)(2,1)S(1)} all-to-all(bf16[8,64,2048]{2,1,0:T(8,128)(2,1)S(1)} %broadcast_select_fusion), channel_id=1, replica_groups=mesh['sp'=8,'tp'=4] {'sp'}, dimensions={0} | all-to-all | bytes 4194304 | tf_op jit(solution)/shard_map/all_to_all | solution.py:148
  264.1 6.3 %convolution_convert_fusion = bf16[512,2048]{1,0:T(8,128)(2,1)} fusion(bf16[1,512,2048]{2,1,0:T(8,128)(2,1)S(1)} %copy-done, bf16[512,2048]{1,0:T(8,128)(2,1)} %bitcast.78, bf16[1,2048,512]{2,1,0:T(8,128)(2,1)} %param.37, f32[512,512]{1,0:T(8,128)} %fusion.16), kind=kOutput, calls=%fused_computation.25 | convolution fusion | flops 2150105088 | bytes 9437184 | tf_op jit(solution)/shard_map/dot_general | solution.py:154
  270.3 4.5 %all-to-all-start.1 = ((bf16[8,64,2048]{2,1,0:T(8,128)(2,1)}), bf16[8,64,2048]{2,1,0:T(8,128)(2,1)}, u32[]{:S(2)}, u32[]{:S(2)}) async-start(bf16[8,64,2048]{2,1,0:T(8,128)(2,1)} %bitcast.76), calls=%async_computation.1 | async-start | bytes 4194304 | tf_op jit(solution)/shard_map/all_to_all | solution.py:157
  276.7 45.4 %all-to-all-done.1 = bf16[8,64,2048]{2,1,0:T(8,128)(2,1)} async-done(((bf16[8,64,2048]{2,1,0:T(8,128)(2,1)}), bf16[8,64,2048]{2,1,0:T(8,128)(2,1)}, u32[]{:S(2)}, u32[]{:S(2)}) %all-to-all-start.1) | async-done | bytes 2097184 | tf_op jit(solution)/shard_map/all_to_all | solution.py:157
  322.1 10.7 %gather_fusion.1 = bf16[1024,2048]{1,0:T(8,128)(2,1)} fusion(bf16[512,2048]{1,0:T(8,128)(2,1)} %bitcast.24, s32[1024]{0:T(1024)S(1)} %broadcast_clamp_fusion), kind=kCustom, calls=%fused_computation.1 | custom fusion | bytes 8392704 | tf_op jit(solution)/shard_map/gather | solution.py:165
  332.8 8.3 %reshape.441 = f32[256,4,2048]{2,1,0:T(4,128)} reshape(bf16[1024,2048]{1,0:T(8,128)(2,1)} %gather_fusion.1) | data formatting | bytes 12582912 | tf_op jit(solution)/shard_map/convert_element_type | solution.py:165
  341.1 11.4 %multiply_reduce_fusion.1 = f32[256,2048]{1,0:T(8,128)} fusion(f32[256,4,2048]{2,1,0:T(4,128)} %reshape.441, f32[256,4]{1,0:T(8,128)S(1)} %copy.55), kind=kLoop, calls=%fused_computation.24 | loop fusion | flops 3670016 | bytes 10489856 | tf_op jit(solution)/shard_map/reduce_sum | solution.py:167
  352.5 3.7 fusion.12
  356.2 23.9 %reduce-scatter.2.cloned.1.call-done = bf16[64,2048]{1,0:T(8,128)(2,1)} async-done(((bf16[256,2048]{1,0:T(8,128)(2,1)}), bf16[64,2048]{1,0:T(8,128)(2,1)}) %reduce-scatter.2.cloned.1.call-update) | async-done | bytes 262160 | tf_op jit(solution)/shard_map/reduce_scatter | solution.py:175
  (82 shorter events, 25.2 us)
Async XLA Ops:
  6.5 257.5 %copy-start = (bf16[1,512,2048]{2,1,0:T(8,128)(2,1)S(1)}, bf16[1,512,2048]{2,1,0:T(8,128)(2,1)}, u32[]{:S(2)}) copy-start(bf16[1,512,2048]{2,1,0:T(8,128)(2,1)} %param.38) | copy-start | bytes 6291460
  6.5 7.6 %copy-start.6 = (bf16[256,256]{1,0:T(8,128)(2,1)S(1)}, bf16[256,256]{1,0:T(8,128)(2,1)}, u32[]{:S(2)}) copy-start(bf16[256,256]{1,0:T(8,128)(2,1)} %param.25) | copy-start | bytes 393220
  6.5 8.3 %copy-start.8 = (s32[256]{0:T(256)S(1)}, s32[256]{0:T(256)}, u32[]{:S(2)}) copy-start(s32[256]{0:T(256)} %param.29) | copy-start | bytes 3076
  6.5 45.0 %all-gather.5.cloned.1.call-start = ((), (), s32[]{:S(2)}) async-start(), calls=%async_computation.3 | async-start | bytes 1179648 | tf_op jit(solution)/shard_map/all_gather | solution.py:91
  8.4 83.7 %all-gather.7.cloned.1.call-start = ((), (), s32[]{:S(2)}) async-start(), calls=%async_computation.4 | async-start | bytes 1179648 | tf_op jit(solution)/shard_map/all_gather | solution.py:71
  10.1 133.4 %all-gather.9.cloned.1.call-start = ((), (), s32[]{:S(2)}) async-start(), calls=%async_computation.5 | async-start | bytes 2359296 | tf_op jit(solution)/shard_map/all_gather | solution.py:93
  12.0 186.5 %all-reduce.2.cloned.1.call-start = ((), (), s32[]{:S(2)}) async-start(), calls=%async_computation.6 | async-start | bytes 2097152 | tf_op jit(solution)/shard_map/psum | solution.py:124
  92.0 51.5 %copy-start.13 = (f32[4]{0:T(128)S(1)}, f32[4]{0:T(128)}, u32[]{:S(2)}) copy-start(f32[4]{0:T(128)} %param.30) | copy-start | bytes 52
  92.0 3.2 copy-start.5
  143.5 16.8 %copy-start.11 = (f32[128]{0:T(128)S(1)}, f32[128]{0:T(128)}, u32[]{:S(2)}) copy-start(f32[128]{0:T(128)} %param.31) | copy-start | bytes 1540
  160.4 38.1 %copy-start.1 = (bf16[256,2048]{1,0:T(8,128)(2,1)S(1)}, bf16[256,2048]{1,0:T(8,128)(2,1)}, u32[]{:S(2)}) copy-start(bf16[256,2048]{1,0:T(8,128)(2,1)} %param.23) | copy-start | bytes 3145732
  164.6 37.0 %copy-start.9 = (f32[2048]{0:T(1024)S(1)}, f32[2048]{0:T(1024)}, u32[]{:S(2)}) copy-start(f32[2048]{0:T(1024)} %param.33) | copy-start | bytes 24580
  198.5 3.1 copy-start.2
  198.5 3.1 copy-start.3
  207.3 54.5 %copy-start.12 = (bf16[1,2048,512]{2,1,0:T(8,128)(2,1)S(1)}, bf16[1,2048,512]{2,1,0:T(8,128)(2,1)}, u32[]{:S(2)}) copy-start(bf16[1,2048,512]{2,1,0:T(8,128)(2,1)} %param.36) | copy-start | bytes 6291460
  260.5 1.3 copy-start.4
  270.3 4.7 %copy-start.7 = (s32[256,4]{0,1:T(4,128)S(1)}, s32[256,4]{0,1:T(4,128)}, u32[]{:S(2)}) copy-start(s32[256,4]{0,1:T(4,128)} %param.34) | copy-start | bytes 12292
  270.3 4.7 %copy-start.10 = (f32[256,4]{0,1:T(4,128)S(1)}, f32[256,4]{0,1:T(4,128)}, u32[]{:S(2)}) copy-start(f32[256,4]{0,1:T(4,128)} %param.35) | copy-start | bytes 12292
  270.3 51.7 %all-to-all-start.1 = ((bf16[8,64,2048]{2,1,0:T(8,128)(2,1)}), bf16[8,64,2048]{2,1,0:T(8,128)(2,1)}, u32[]{:S(2)}, u32[]{:S(2)}) async-start(bf16[8,64,2048]{2,1,0:T(8,128)(2,1)} %bitcast.76), calls=%async_computation.1 | async-start | bytes 4194304 | tf_op jit(solution)/shard_map/all_to_all | solution.py:157
  274.8 105.3 %reduce-scatter.2.cloned.1.call-start = ((), (), s32[]{:S(2)}) async-start(), calls=%async_computation.7 | async-start | bytes 1310720 | tf_op jit(solution)/shard_map/reduce_scatter | solution.py:175
Sparse Core Ops, SparseCore 0:
  9.4 42.1 all-gather.4
  53.6 38.3 all-gather.6
  94.1 49.3 all-gather.8
  164.0 34.4 all-reduce.1
  356.3 23.7 reduce-scatter.1
where the time goes:
time: 389 us
  waiting for transfers between devices  191 us (49%)
  blocking collectives  75.5 us (19%)
  matrix products  38.2 us (10%)
  local copies, waits for them, and re-layouts  32.8 us (8%)
  other arithmetic  30.8 us (8%)
  between operations  15.1 us (4%)
  starting transfers between devices  4.67 us (1%)
    all_to_all x1, blocking collectives, local(): lax.all_to_all(outgoing, 'sp', split_axis=0, concat_axis=0, tiled=True)  53.2 us
    all_to_all x1, waiting for transfers between devices, local(): lax.all_to_all(result.reshape(seq_size, item_count, model_width), 'sp', s...  45.4 us
    all_gather x1, waiting for transfers between devices, local(): key_second = lax.all_gather(key_two, 'sp', axis=0, tiled=True)  40.5 us
    all_gather x1, waiting for transfers between devices, local(): value_block = lax.all_gather(values, 'sp', axis=0, tiled=True)  39 us
    psum x1, waiting for transfers between devices, local(): lax.psum(proj_term.astype(jnp.bfloat16), 'tp').astype(jnp.float32)  33.9 us
    reduce_scatter x1, waiting for transfers between devices, local(): lax.psum_scatter((routed + shared_out).astype(jnp.bfloat16), 'tp', scatte...  23.9 us
    all_gather x1, blocking collectives, local(): apply_key_docs = lax.all_gather(documents, 'sp', axis=0, tiled=True)  22.3 us
    dot_general x3, matrix products, scores(): jnp.einsum('qhd,khd->hqk', query_block, keyed, preferred_element_type=jnp...  11.5 us
  transfers between devices with their start and end apart: 6, of which 6 were waited for; matrix products, arithmetic and copies ran while one was open for 6% of the time, Pallas kernels for 0%

commit v1 on v0

v1 whole, which is shorter than its diff:
```python
import functools

import jax
import jax.numpy as jnp
from jax import lax
from jax.experimental import pallas as pl
from jax.experimental.pallas import tpu as pltpu
from jax.sharding import PartitionSpec as P

NEG_FILL = -1e30
HEAD_SCALE = 0.8


def rms_scale(values_in, eps_value):
    return lax.rsqrt(jnp.mean(values_in * values_in, axis=-1, keepdims=True) + eps_value)


def row_width(count):
    width = 1
    while (2 * width) * (2 * width) <= count:
        width *= 2
    return width if count % width == 0 else 1


def gather_kernel(count, wide, k1, k2, val, doc, k1_all, k2_all, val_all, doc_all,
                  own_sem, z_send, z_recv, x_send, x_recv, d_send, d_recv):
    tall = count // wide
    me = lax.axis_index("sp")
    row, col = me // wide, me % wide
    pieces = ((k1, k1_all), (k2, k2_all), (val, val_all))

    barrier = pltpu.get_barrier_semaphore()
    for off in range(1, count):
        pl.semaphore_signal(
            barrier, inc=1, device_id={"sp": lax.rem(me + off, count)},
            device_id_type=pl.DeviceIdType.MESH,
        )
    pl.semaphore_wait(barrier, count - 1)

    def remote(src, dst, send, recv, target):
        return pltpu.make_async_remote_copy(
            src_ref=src, dst_ref=dst, send_sem=send, recv_sem=recv,
            device_id={"sp": target}, device_id_type=pl.DeviceIdType.MESH,
        )

    def hop(way, hops, piece):
        src, everything = pieces[piece]
        step = 1 if way == 0 else -1
        origin = (row + step - step * hops) * wide + col
        slot = everything.at[origin]
        source = src if hops == 1 else slot
        return remote(source, slot, z_send.at[way, hops, piece], z_recv.at[way, hops, piece],
                      me + step * wide)

    def arrived_hop(way, hops, piece):
        everything = pieces[piece][1]
        step = 1 if way == 0 else -1
        slot = everything.at[me - step * hops * wide]
        return remote(slot, slot, z_send.at[way, hops, piece], z_recv.at[way, hops, piece],
                      me - step * wide)

    def across(way, hops, piece, off, landing):
        src, everything = pieces[piece]
        step = 1 if way == 0 else -1
        from_col = lax.rem(col + wide - off, wide) if landing else col
        slot = everything.at[(row - step * hops) * wide + from_col]
        source = src if hops == 0 and not landing else slot
        target = row * wide + (from_col if landing else lax.rem(col + off, wide))
        return remote(source, slot, x_send.at[way, hops, piece, off],
                      x_recv.at[way, hops, piece, off], target)

    offsets = range(1, wide)
    ways = (0, 1)

    def has(way, hops):
        return row >= hops if way == 0 else row + hops < tall

    def open_end(way):
        return row + 1 < tall if way == 0 else row > 0

    doc_copies = [
        remote(doc, doc_all.at[me], d_send.at[off], d_recv.at[off], lax.rem(me + off, count))
        for off in range(1, count)
    ]
    own_copies = [
        pltpu.make_async_copy(src, everything.at[me], own_sem.at[piece])
        for piece, (src, everything) in enumerate(pieces + ((doc, doc_all),))
    ]
    for copy in doc_copies:
        copy.start()
    for piece in range(3):
        for way in ways:
            @pl.when(open_end(way))
            def _(way=way, piece=piece):
                hop(way, 1, piece).start()
        for off in offsets:
            across(0, 0, piece, off, False).start()
    for copy in own_copies:
        copy.start()
    for hops in range(1, tall):
        for piece in range(3):
            for way in ways:
                @pl.when(has(way, hops))
                def _(way=way, piece=piece, hops=hops):
                    arrived_hop(way, hops, piece).wait_recv()
                    if hops + 1 < tall:
                        @pl.when(open_end(way))
                        def _():
                            hop(way, hops + 1, piece).start()
                    for off in offsets:
                        across(way, hops, piece, off, False).start()
    for piece in range(3):
        for off in offsets:
            across(0, 0, piece, off, True).wait_recv()
            across(0, 0, piece, off, False).wait_send()
        for way in ways:
            @pl.when(open_end(way))
            def _(way=way, piece=piece):
                hop(way, 1, piece).wait_send()
    for hops in range(1, tall):
        for piece in range(3):
            for way in ways:
                @pl.when(has(way, hops))
                def _(way=way, piece=piece, hops=hops):
                    if hops + 1 < tall:
                        @pl.when(open_end(way))
                        def _():
                            hop(way, hops + 1, piece).wait_send()
                    for off in offsets:
                        across(way, hops, piece, off, True).wait_recv()
                        across(way, hops, piece, off, False).wait_send()
    for copy in own_copies:
        copy.wait()
    for off in range(1, count):
        sender = lax.rem(me + count - off, count)
        slot = doc_all.at[sender]
        remote(slot, slot, d_send.at[off], d_recv.at[off], sender).wait_recv()
        doc_copies[off - 1].wait_send()


def gather_all(key_one, key_two, values, documents):
    count = lax.axis_size("sp")
    wide = row_width(count)
    tall = count // wide
    dma = pltpu.SemaphoreType.DMA
    rows = key_one.shape[0]
    doc = documents.reshape(1, rows)
    outs = [jax.ShapeDtypeStruct((count,) + a.shape, a.dtype)
            for a in (key_one, key_two, values, doc)]
    vmem = pl.BlockSpec(memory_space=pltpu.VMEM)
    sent = (count - 1) * (key_one.size + key_two.size + values.size) * 2
    return pl.pallas_call(
        functools.partial(gather_kernel, count, wide),
        out_shape=outs,
        in_specs=[vmem] * 4,
        out_specs=[vmem] * 4,
        scratch_shapes=[
            dma((4,)), dma((2, tall, 3)), dma((2, tall, 3)),
            dma((2, tall, 3, wide)), dma((2, tall, 3, wide)), dma((count,)), dma((count,)),
        ],
        compiler_params=pltpu.CompilerParams(collective_id=0, has_side_effects=True,
                                             vmem_limit_bytes=40 * 1024 * 1024),
        cost_estimate=pl.CostEstimate(flops=0, bytes_accessed=sent, transcendentals=0),
        name="gather_keys",
    )(key_one, key_two, values, doc)


def local(
    resid,
    query_one,
    query_two,
    key_one,
    key_two,
    values,
    documents,
    mix_lambda,
    head_gain,
    out_weight,
    ffn_gain,
    routes,
    route_weight,
    expert_gate,
    expert_up,
    expert_down,
    shared_gate,
    shared_up,
    shared_down,
):
    tok_rows = query_one.shape[0]
    head_count = mix_lambda.shape[0]
    head_width = query_one.shape[1] // head_count
    value_width = values.shape[1] // head_count
    model_width = resid.shape[1]
    score_scale = head_width ** (-0.5)
    seq_size = lax.axis_size("sp")
    tp_size = lax.axis_size("tp")
    query_pos = lax.axis_index("sp") * tok_rows + jnp.arange(tok_rows, dtype=jnp.int32)
    query_first = query_one.reshape(tok_rows, head_count, head_width)
    query_second = query_two.reshape(tok_rows, head_count, head_width)
    lambda_col = mix_lambda[:, None, None]
    key_first, key_second, value_block, key_docs = gather_all(
        key_one, key_two, values, documents
    )
    key_total = seq_size * tok_rows
    key_docs = key_docs.reshape(key_total)
    key_pos = jnp.arange(key_total, dtype=jnp.int32)
    allowed = (
        (key_pos[None, :] <= query_pos[:, None]) & (key_docs[None, :] == documents[:, None])
    )[None]

    def probs(query_block, key_block):
        keyed = key_block.reshape(key_total, head_count, head_width)
        raw = (
            jnp.einsum("qhd,khd->hqk", query_block, keyed, preferred_element_type=jnp.float32)
            * score_scale
        )
        masked = jnp.where(allowed, raw, NEG_FILL)
        fresh = jnp.exp(masked - jnp.max(masked, axis=-1, keepdims=True))
        return fresh / jnp.sum(fresh, axis=-1, keepdims=True)

    weights = (
        probs(query_first, key_first) - lambda_col * probs(query_second, key_second)
    ).astype(jnp.bfloat16)
    valued = value_block.reshape(key_total, head_count, value_width)
    head_out = jnp.einsum("hqk,khv->hqv", weights, valued, preferred_element_type=jnp.float32)
    normed_heads = (head_out * rms_scale(head_out, 1e-05) * head_gain * HEAD_SCALE).astype(
        jnp.bfloat16
    )
    attn_rows = normed_heads.transpose(1, 0, 2).reshape(tok_rows, head_count * value_width)
    share_rows = tok_rows // tp_size
    own_start = lax.axis_index("tp") * share_rows
    proj_term = jnp.dot(attn_rows, out_weight, preferred_element_type=jnp.float32)
    projected = lax.psum(proj_term.astype(jnp.bfloat16), "tp").astype(jnp.float32)
    mixed_all = resid.astype(jnp.float32) + projected
    normed_all = (mixed_all * rms_scale(mixed_all, 1e-06) * ffn_gain).astype(jnp.bfloat16)
    mixed_own = lax.dynamic_slice_in_dim(mixed_all, own_start, share_rows, 0)
    route_slots = routes.shape[1]
    capacity = max(2, 2 * tok_rows * route_slots // (seq_size * tp_size))
    tp_index = lax.axis_index("tp")
    group_experts = jnp.arange(seq_size, dtype=jnp.int32) * tp_size + tp_index
    named = routes[:, :, None] == group_experts[None, None, :]
    token_weight = jnp.sum(jnp.where(named, route_weight[:, :, None], 0.0), axis=1)
    is_named = jnp.any(named, axis=1)
    token_pos = jnp.arange(tok_rows, dtype=jnp.int32)
    earlier = (token_pos[None, :] < token_pos[:, None]).astype(jnp.bfloat16)
    rank = jnp.dot(earlier, is_named.astype(jnp.bfloat16), preferred_element_type=jnp.float32)
    place = jnp.where(is_named, rank.astype(jnp.int32), -1)
    slot_total = seq_size * capacity
    in_slot = place[:, :, None] == jnp.arange(capacity, dtype=jnp.int32)[None, None, :]
    pick = in_slot.reshape(tok_rows, slot_total).astype(jnp.bfloat16)
    combine = jnp.where(in_slot, token_weight[:, :, None], 0.0).reshape(tok_rows, slot_total)
    combine_high = lax.reduce_precision(combine, 8, 7)
    combine_low = (combine - combine_high).astype(jnp.bfloat16)
    outgoing = lax.dot_general(
        pick, normed_all, (((0,), (0,)), ((), ())), preferred_element_type=jnp.float32
    ).astype(jnp.bfloat16).reshape(seq_size, capacity, model_width)
    arrived = lax.all_to_all(outgoing, "sp", split_axis=0, concat_axis=0, tiled=True)
    item_count = arrived.shape[1]
    flat_rows = arrived.reshape(seq_size * item_count, model_width)
    gate_part = jnp.dot(flat_rows, expert_gate[0], preferred_element_type=jnp.float32)
    up_part = jnp.dot(flat_rows, expert_up[0], preferred_element_type=jnp.float32)
    hidden = (jax.nn.silu(gate_part) * up_part).astype(jnp.bfloat16)
    result = jnp.dot(hidden, expert_down[0], preferred_element_type=jnp.float32).astype(
        jnp.bfloat16
    )
    returned = lax.all_to_all(
        result.reshape(seq_size, item_count, model_width),
        "sp",
        split_axis=0,
        concat_axis=0,
        tiled=True,
    )
    returned_flat = returned.reshape(slot_total, model_width)
    routed = jnp.dot(
        combine_high.astype(jnp.bfloat16), returned_flat, preferred_element_type=jnp.float32
    ) + jnp.dot(combine_low, returned_flat, preferred_element_type=jnp.float32)
    shared_act = (
        jax.nn.silu(jnp.dot(normed_all, shared_gate, preferred_element_type=jnp.float32))
        * jnp.dot(normed_all, shared_up, preferred_element_type=jnp.float32)
    ).astype(jnp.bfloat16)
    shared_out = jnp.dot(shared_act, shared_down, preferred_element_type=jnp.float32)
    ffn_own = lax.psum_scatter(
        (routed + shared_out).astype(jnp.bfloat16), "tp", scatter_dimension=0, tiled=True
    ).astype(jnp.float32)
    return (mixed_own + ffn_own).astype(jnp.bfloat16)


def solution(mesh):
    placed = (
        P("sp", None),
        P("sp", "tp"),
        P("sp", "tp"),
        P("sp", "tp"),
        P("sp", "tp"),
        P("sp", "tp"),
        P("sp"),
        P("tp"),
        P(),
        P("tp", None),
        P(),
        P("sp", None),
        P("sp", None),
        P(("sp", "tp"), None, None),
        P(("sp", "tp"), None, None),
        P(("sp", "tp"), None, None),
        P(None, "tp"),
        P(None, "tp"),
        P("tp", None),
    )
    return jax.shard_map(
        local, mesh=mesh, in_specs=placed, out_specs=P(("sp", "tp"), None), check_vma=False
    )
```

time: 389 us -> 300 us (0.77)
  waiting for transfers between devices: 191 us -> 104 us
  Pallas kernels: 0 us -> 53.5 us
  other arithmetic: 30.8 us -> 8.28 us
  blocking collectives: 75.5 us -> 53.2 us
  local copies, waits for them, and re-layouts: 32.8 us -> 21.7 us
    all_gather x3 -> x0, waiting for transfers between devices: 88.1 us -> none  [the longest x1 40.5 us: local(): key_second = lax.all_gather(key_two, 'sp', axis=0, tiled=True)]
    pallas_call x0 -> x1, Pallas kernels: none -> 53.5 us  [gather_all(): pl.pallas_call(functools.partial(gather_kernel, count, wide), out_shape=o...]
    all_gather x1 -> x0, blocking collectives: 22.3 us -> none  [local(): apply_key_docs = lax.all_gather(documents, 'sp', axis=0, tiled=True)]
    reduce_sum x4 -> x1, other arithmetic: 17.2 us -> 0.08 us  [local(): jnp.sum(jnp.where(named, route_weight[:, :, None], 0.0), axis=1)]
    gather x2 -> x0, local copies, waits for them, and re-layouts: 14 us -> none  [the longest x1 10.7 us: local(): picked = returned_flat[jnp.maximum(slot_id, 0)].astype(jnp.float32)]
    convert_element_type x1 -> x0, local copies, waits for them, and re-layouts: 8.31 us -> none  [local(): picked = returned_flat[jnp.maximum(slot_id, 0)].astype(jnp.float32)]
    reshape x3, local copies, waits for them, and re-layouts: 0.36 us -> 7.9 us  [the longest x1 4 us: local(): valued = value_block.reshape(key_total, head_count, value_width)]
    sub x0 -> x1, matrix products: none -> 7.38 us  [probs(): fresh = jnp.exp(masked - jnp.max(masked, axis=-1, keepdims=True))]
  transfers between devices with their start and end apart: 6 -> 3, of which waited for: 6 -> 3; matrix products, arithmetic and copies ran while one was open for 6% -> 1% of each run, Pallas kernels for 0% -> 0%
where the time goes in v1:
time: 300 us
  waiting for transfers between devices  104 us (35%)
  Pallas kernels  53.5 us (18%)
  blocking collectives  53.2 us (18%)
  matrix products  41.1 us (14%)
  local copies, waits for them, and re-layouts  21.7 us (7%)
  between operations  13.6 us (5%)
  other arithmetic  8.28 us (3%)
  starting transfers between devices  4.51 us (2%)
    pallas_call x1, Pallas kernels, gather_all(): pl.pallas_call(functools.partial(gather_kernel, count, wide), out_shape=o...  53.5 us
    all_to_all x1, blocking collectives, local(): lax.all_to_all(outgoing, 'sp', split_axis=0, concat_axis=0, tiled=True)  53.2 us
    all_to_all x1, waiting for transfers between devices, local(): lax.all_to_all(result.reshape(seq_size, item_count, model_width), 'sp', s...  45.6 us
    psum x1, waiting for transfers between devices, local(): lax.psum(proj_term.astype(jnp.bfloat16), 'tp').astype(jnp.float32)  34.2 us
    reduce_scatter x1, waiting for transfers between devices, local(): lax.psum_scatter((routed + shared_out).astype(jnp.bfloat16), 'tp', scatte...  23.9 us
    dot_general x1, matrix products, local(): jnp.einsum('hqk,khv->hqv', weights, valued, preferred_element_type=jnp.fl...  9.83 us
    unnamed x38, local copies, waits for them, and re-layouts  9.28 us
    sub x1, matrix products, probs(): fresh = jnp.exp(masked - jnp.max(masked, axis=-1, keepdims=True))  7.38 us
  transfers between devices with their start and end apart: 3, of which 3 were waited for; matrix products, arithmetic and copies ran while one was open for 1% of the time, Pallas kernels for 0%

profile of v1, /device:TPU:0, one launch (start us, length us, event | category | flops | bytes accessed | tf_op | source)
XLA Modules:
  0.0 299.6 jit_solution(4169222994849956009)
XLA Ops:
  12.2 53.5 %gather_keys.1 = (bf16[8,256,256]{2,1,0:T(8,128)(2,1)S(1)}, bf16[8,256,256]{2,1,0:T(8,128)(2,1)S(1)}, bf16[8,256,512]{2,1,0:T(8,128)(2,1)S(1)}, s32[8,1,256]{2,1,0:T(1,128)S(1)}) custom-call(bf16[256,256]{1,0:T(8,128)(2,1)S(1)} %copy-done.4, bf16[256,256]{1,0:T(8,128)(2,1)S(1)} %copy-done.5, bf16[256,512]{1,0:T(8,128)(2,1)S(1)} %copy-done.3, ...), custom_call_target="tpu_custom_call" | custom-call | bytes 3670016 | tf_op jit(solution)/shard_map/gather_keys/pallas_call | solution.py:152
  65.7 1.3 copy-done.1
  68.0 2.7 copy.36
  70.6 2.3 reshape.137
  73.0 1.8 copy.38
  74.8 1.6 reshape.139
  76.3 4.0 %reshape.141 = bf16[2048,4,128]{2,1,0:T(4,128)(2,1)} reshape(bf16[8,256,512]{2,1,0:T(8,128)(2,1)} %copy-done.1) | data formatting | bytes 4194304 | tf_op jit(solution)/shard_map/reshape | solution.py:224
  81.6 7.4 %fusion.63 = (f32[4,256]{1,0:T(4,128)S(1)}, f32[4,256,2048]{1,2,0:T(8,128)}) fusion(pred[256,2048]{0,1:T(8,128)(4,1)} %fusion.20, bf16[2048,4,64]{0,2,1:T(8,128)(2,1)} %reshape.137, bf16[256,4,64]{0,2,1:T(8,128)(2,1)S(1)} %bitcast.103), kind=kOutput, calls=%fused_computation.85 | convolution fusion | flops 276826112 | bytes 10096640 | tf_op jit(solution)/shard_map/sub | solution.py:218
  89.0 9.8 %multiply_reduce_fusion.1 = (f32[4,256]{1,0:T(4,128)S(1)}, f32[4,256,128]{1,2,0:T(8,128)}) fusion(f32[4,256,2048]{1,2,0:T(8,128)} %get-tuple-element.16, f32[4]{0:T(128)S(1)} %copy-done.17, f32[4,256]{1,0:T(4,128)S(1)} %get-tuple-element.15, bf16[2048,4,128]{2,1,0:T(4,128)(2,1)} %reshape.141, pred[256,2048]{0,1:T(8,128)(4,1)} %fusion.20, ...), kind=kOutput, calls=%fused_computation.55 | convolution fusion | flops 822350848 | bytes 12722192 | tf_op jit(solution)/shard_map/hqk,khv->hqv/dot_general | solution.py:225
  100.0 3.4 %convolution_convert_fusion.2 = bf16[256,2048]{1,0:T(8,128)(2,1)} fusion(bf16[256,512]{0,1:T(8,128)(2,1)S(1)} %bitcast.101, bf16[512,2048]{1,0:T(8,128)(2,1)} %param.28), kind=kOutput, calls=%fused_computation.23 | convolution fusion | flops 537395200 | bytes 3407872 | tf_op jit(solution)/shard_map/dot_general | solution.py:232
  104.0 34.2 %all-reduce.2.cloned.1.call-done = bf16[256,2048]{1,0:T(8,128)(2,1)} async-done(((bf16[256,2048]{1,0:T(8,128)(2,1)}), bf16[256,2048]{1,0:T(8,128)(2,1)}) %all-reduce.2.cloned.1.call-update) | async-done | bytes 1048592 | tf_op jit(solution)/shard_map/psum | solution.py:233
  138.2 3.1 %convert_add_fusion = (f32[256,2048]{1,0:T(8,128)}, f32[256]{0:T(256)S(1)}) fusion(bf16[256,2048]{1,0:T(8,128)(2,1)} %all-reduce.2.cloned.1.call-done, bf16[256,2048]{1,0:T(8,128)(2,1)S(1)} %copy-done.8), kind=kLoop, calls=%fused_computation.33 | loop fusion | flops 2621184 | bytes 4195328 | tf_op jit(solution)/shard_map/add | solution.py:234
  142.6 53.2 %all_to_all.10 = bf16[8,64,2048]{2,1,0:T(8,128)(2,1)S(1)} all-to-all(bf16[8,64,2048]{2,1,0:T(8,128)(2,1)S(1)} %bitcast.97), channel_id=1, replica_groups=mesh['sp'=8,'tp'=4] {'sp'}, dimensions={0} | all-to-all | bytes 4194304 | tf_op jit(solution)/shard_map/all_to_all | solution.py:257
  195.8 1.3 copy-done.11
  197.1 2.3 fusion.17
  199.4 6.2 %convolution_convert_fusion.1 = bf16[512,2048]{1,0:T(8,128)(2,1)} fusion(bf16[1,512,2048]{2,1,0:T(8,128)(2,1)S(1)} %copy-done, bf16[512,2048]{1,0:T(8,128)(2,1)} %bitcast.100, bf16[1,2048,512]{2,1,0:T(8,128)(2,1)} %param.33, f32[512,512]{1,0:T(8,128)} %fusion.17), kind=kOutput, calls=%fused_computation.18 | convolution fusion | flops 2150105088 | bytes 9437184 | tf_op jit(solution)/shard_map/dot_general | solution.py:263
  205.6 4.5 %all-to-all-start.1 = ((bf16[8,64,2048]{2,1,0:T(8,128)(2,1)}), bf16[8,64,2048]{2,1,0:T(8,128)(2,1)}, u32[]{:S(2)}, u32[]{:S(2)}) async-start(bf16[8,64,2048]{2,1,0:T(8,128)(2,1)} %bitcast.98), calls=%async_computation.1 | async-start | bytes 4194304 | tf_op jit(solution)/shard_map/all_to_all | solution.py:266
  210.2 1.5 fusion.68
  211.7 45.6 %all-to-all-done.1 = bf16[8,64,2048]{2,1,0:T(8,128)(2,1)} async-done(((bf16[8,64,2048]{2,1,0:T(8,128)(2,1)}), bf16[8,64,2048]{2,1,0:T(8,128)(2,1)}, u32[]{:S(2)}, u32[]{:S(2)}) %all-to-all-start.1) | async-done | bytes 2097184 | tf_op jit(solution)/shard_map/all_to_all | solution.py:266
  257.3 2.3 convolution_bitcast_fusion
  259.6 3.7 %fusion.12 = f32[256,2048]{1,0:T(8,128)} fusion(f32[256,2048]{1,0:T(8,128)S(1)} %convolution_bitcast_fusion, bf16[8,64,2048]{2,1,0:T(8,128)(2,1)} %all-to-all-done.1, f32[256,8]{0,1:T(8,128)S(1)} %fusion.53, s32[256,8]{0,1:T(8,128)S(1)} %fusion.28), kind=kOutput, calls=%fused_computation.22 | convolution fusion | flops 537919488 | bytes 6307840 | tf_op jit(solution)/shard_map/dot_general | solution.py:274
  263.3 3.7 %fusion.13 = bf16[256,2048]{1,0:T(8,128)(2,1)} fusion(f32[256,2048]{1,0:T(8,128)} %fusion.12, bf16[128,2048]{1,0:T(8,128)(2,1)} %param.37, bf16[256,2048]{1,0:T(8,128)(2,1)S(1)} %multiply_convert_fusion, bf16[2048,128]{1,0:T(8,128)(2,1)} %param.36, f32[256,128]{1,0:T(8,128)S(1)} %fusion.68), kind=kOutput, calls=%fused_computation.24 | convolution fusion | flops 269680640 | bytes 5373952 | tf_op jit(solution)/shard_map/dot_general | solution.py:281
  267.0 23.9 %reduce-scatter.2.cloned.1.call-done = bf16[64,2048]{1,0:T(8,128)(2,1)} async-done(((bf16[256,2048]{1,0:T(8,128)(2,1)}), bf16[64,2048]{1,0:T(8,128)(2,1)}) %reduce-scatter.2.cloned.1.call-update) | async-done | bytes 262160 | tf_op jit(solution)/shard_map/reduce_scatter | solution.py:282
  290.9 1.9 add_convert_fusion
  (54 shorter events, 11.0 us)
Async XLA Ops:
  6.5 192.8 %copy-start = (bf16[1,512,2048]{2,1,0:T(8,128)(2,1)S(1)}, bf16[1,512,2048]{2,1,0:T(8,128)(2,1)}, u32[]{:S(2)}) copy-start(bf16[1,512,2048]{2,1,0:T(8,128)(2,1)} %param.34) | copy-start | bytes 6291460
  6.5 131.6 %all-reduce.2.cloned.1.call-start = ((), (), s32[]{:S(2)}) async-start(), calls=%async_computation.3 | async-start | bytes 2097152 | tf_op jit(solution)/shard_map/psum | solution.py:233
  8.7 1.0 copy-start.3
  9.7 0.9 copy-start.4
  10.6 0.9 copy-start.5
  11.5 0.7 copy-start.6
  65.6 1.3 copy-start.1
  67.0 1.0 copy-start.2
  76.3 4.0 %copy-start.7 = (s32[256]{0:T(256)S(1)}, s32[256]{0:T(256)}, u32[]{:S(2)}) copy-start(s32[256]{0:T(256)} %param.25) | copy-start | bytes 3076
  81.6 7.4 %copy-start.17 = (f32[4]{0:T(128)S(1)}, f32[4]{0:T(128)}, u32[]{:S(2)}) copy-start(f32[4]{0:T(128)} %param.26) | copy-start | bytes 52
  89.0 9.8 %copy-start.15 = (f32[128]{0:T(128)S(1)}, f32[128]{0:T(128)}, u32[]{:S(2)}) copy-start(f32[128]{0:T(128)} %param.27) | copy-start | bytes 1540
  100.0 3.5 %copy-start.12 = (s32[256,4]{0,1:T(4,128)S(1)}, s32[256,4]{0,1:T(4,128)}, u32[]{:S(2)}) copy-start(s32[256,4]{0,1:T(4,128)} %param.30) | copy-start | bytes 12292
  100.0 38.1 %copy-start.8 = (bf16[256,2048]{1,0:T(8,128)(2,1)S(1)}, bf16[256,2048]{1,0:T(8,128)(2,1)}, u32[]{:S(2)}) copy-start(bf16[256,2048]{1,0:T(8,128)(2,1)} %param.19) | copy-start | bytes 3145732
  104.0 37.3 %copy-start.13 = (f32[2048]{0:T(1024)S(1)}, f32[2048]{0:T(1024)}, u32[]{:S(2)}) copy-start(f32[2048]{0:T(1024)} %param.29) | copy-start | bytes 24580
  138.2 3.1 %copy-start.9 = (bf16[256,2048]{1,0:T(8,128)(2,1)S(1)}, bf16[256,2048]{1,0:T(8,128)(2,1)}, u32[]{:S(2)}) copy-start(bf16[256,2048]{1,0:T(8,128)(2,1)} %param.19) | copy-start | bytes 3145732
  138.2 3.1 %copy-start.10 = (bf16[256,2048]{1,0:T(8,128)(2,1)S(1)}, bf16[256,2048]{1,0:T(8,128)(2,1)}, u32[]{:S(2)}) copy-start(bf16[256,2048]{1,0:T(8,128)(2,1)} %all-reduce.2.cloned.1.call-done) | copy-start | bytes 3145732
  142.6 54.5 %copy-start.16 = (bf16[1,2048,512]{2,1,0:T(8,128)(2,1)S(1)}, bf16[1,2048,512]{2,1,0:T(8,128)(2,1)}, u32[]{:S(2)}) copy-start(bf16[1,2048,512]{2,1,0:T(8,128)(2,1)} %param.32) | copy-start | bytes 6291460
  195.7 1.3 copy-start.11
  205.6 4.5 %copy-start.14 = (f32[256,4]{0,1:T(4,128)S(1)}, f32[256,4]{0,1:T(4,128)}, u32[]{:S(2)}) copy-start(f32[256,4]{0,1:T(4,128)} %param.31) | copy-start | bytes 12292
  205.6 51.7 %all-to-all-start.1 = ((bf16[8,64,2048]{2,1,0:T(8,128)(2,1)}), bf16[8,64,2048]{2,1,0:T(8,128)(2,1)}, u32[]{:S(2)}, u32[]{:S(2)}) async-start(bf16[8,64,2048]{2,1,0:T(8,128)(2,1)} %bitcast.98), calls=%async_computation.1 | async-start | bytes 4194304 | tf_op jit(solution)/shard_map/all_to_all | solution.py:266
  210.1 80.8 %reduce-scatter.2.cloned.1.call-start = ((), (), s32[]{:S(2)}) async-start(), calls=%async_computation.4 | async-start | bytes 1310720 | tf_op jit(solution)/shard_map/reduce_scatter | solution.py:282
Sparse Core Ops, SparseCore 0:
  103.6 34.5 all-reduce.1
  267.1 23.7 reduce-scatter.1

commit v2 on v1

--- a/solution.py
+++ b/solution.py
@@ -165,6 +165,57 @@
     )(key_one, key_two, values, doc)
 
 
+def swap_kernel(count, spread, src, out, own_sem, send, recv):
+    me = lax.axis_index("tp")
+    barrier = pltpu.get_barrier_semaphore()
+    for off in range(1, count):
+        pl.semaphore_signal(
+            barrier, inc=1, device_id={"tp": lax.rem(me + off, count)},
+            device_id_type=pl.DeviceIdType.MESH,
+        )
+    pl.semaphore_wait(barrier, count - 1)
+
+    def part(index):
+        return src.at[index] if spread else src.at[0]
+
+    copies = []
+    for off in range(1, count):
+        target = lax.rem(me + off, count)
+        copy = pltpu.make_async_remote_copy(
+            src_ref=part(target), dst_ref=out.at[me], send_sem=send.at[off],
+            recv_sem=recv.at[off], device_id={"tp": target},
+            device_id_type=pl.DeviceIdType.MESH,
+        )
+        copy.start()
+        copies.append(copy)
+    own = pltpu.make_async_copy(part(me), out.at[me], own_sem.at[0])
+    own.start()
+    for off in range(1, count):
+        sender = lax.rem(me + count - off, count)
+        pltpu.make_async_remote_copy(
+            src_ref=out.at[sender], dst_ref=out.at[sender], send_sem=send.at[off],
+            recv_sem=recv.at[off], device_id={"tp": sender},
+            device_id_type=pl.DeviceIdType.MESH,
+        ).wait_recv()
+        copies[off - 1].wait_send()
+    own.wait()
+
+
+def swap_tp(parts, collective_id):
+    count = lax.axis_size("tp")
+    dma = pltpu.SemaphoreType.DMA
+    vmem = pl.BlockSpec(memory_space=pltpu.VMEM)
+    return pl.pallas_call(
+        functools.partial(swap_kernel, count, parts.shape[0] == count),
+        out_shape=jax.ShapeDtypeStruct((count,) + parts.shape[1:], parts.dtype),
+        in_specs=[vmem],
+        out_specs=vmem,
+        scratch_shapes=[dma((1,)), dma((count,)), dma((count,))],
+        compiler_params=pltpu.CompilerParams(collective_id=collective_id, has_side_effects=True),
+        name="swap_tp_%d" % collective_id,
+    )(parts)
+
+
 def local(
     resid,
     query_one,
@@ -230,10 +281,13 @@
     share_rows = tok_rows // tp_size
     own_start = lax.axis_index("tp") * share_rows
     proj_term = jnp.dot(attn_rows, out_weight, preferred_element_type=jnp.float32)
-    projected = lax.psum(proj_term.astype(jnp.bfloat16), "tp").astype(jnp.float32)
-    mixed_all = resid.astype(jnp.float32) + projected
-    normed_all = (mixed_all * rms_scale(mixed_all, 1e-06) * ffn_gain).astype(jnp.bfloat16)
-    mixed_own = lax.dynamic_slice_in_dim(mixed_all, own_start, share_rows, 0)
+    proj_parts = swap_tp(
+        proj_term.astype(jnp.bfloat16).reshape(tp_size, share_rows, model_width), 1
+    )
+    resid_own = lax.dynamic_slice_in_dim(resid, own_start, share_rows, 0)
+    mixed_own = resid_own.astype(jnp.float32) + jnp.sum(proj_parts.astype(jnp.float32), axis=0)
+    normed_own = (mixed_own * rms_scale(mixed_own, 1e-06) * ffn_gain).astype(jnp.bfloat16)
+    normed_all = swap_tp(normed_own[None], 2).reshape(tok_rows, model_width)
     route_slots = routes.shape[1]
     capacity = max(2, 2 * tok_rows * route_slots // (seq_size * tp_size))
     tp_index = lax.axis_index("tp")
@@ -279,9 +333,10 @@
         * jnp.dot(normed_all, shared_up, preferred_element_type=jnp.float32)
     ).astype(jnp.bfloat16)
     shared_out = jnp.dot(shared_act, shared_down, preferred_element_type=jnp.float32)
-    ffn_own = lax.psum_scatter(
-        (routed + shared_out).astype(jnp.bfloat16), "tp", scatter_dimension=0, tiled=True
-    ).astype(jnp.float32)
+    ffn_parts = swap_tp(
+        (routed + shared_out).astype(jnp.bfloat16).reshape(tp_size, share_rows, model_width), 3
+    )
+    ffn_own = jnp.sum(ffn_parts.astype(jnp.float32), axis=0)
     return (mixed_own + ffn_own).astype(jnp.bfloat16)
 
 

time: 300 us -> 281 us (0.937)
  waiting for transfers between devices: 104 us -> 46.9 us
  Pallas kernels: 53.5 us -> 99.7 us
  between operations: 13.6 us -> 0.22 us
  other arithmetic: 8.28 us -> 12.4 us
    pallas_call x0 -> x3, Pallas kernels: none -> 46.2 us  [swap_tp(): pl.pallas_call(functools.partial(swap_kernel, count, parts.shape[0] == co...]
    psum x1 -> x0, waiting for transfers between devices: 34.2 us -> none  [local(): lax.psum(proj_term.astype(jnp.bfloat16), 'tp').astype(jnp.float32)]
    reduce_scatter x1 -> x0, waiting for transfers between devices: 23.9 us -> none  [local(): lax.psum_scatter((routed + shared_out).astype(jnp.bfloat16), 'tp', scatte...]
    reduce_sum x0 -> x3, other arithmetic: none -> 4.18 us  [the longest x1 1.43 us: local(): jnp.sum(proj_parts.astype(jnp.float32), axis=0)]
    add x1 -> x0, other arithmetic: 3.05 us -> none  [local(): mixed_all = resid.astype(jnp.float32) + projected]
    unnamed x38 -> x42, local copies, waits for them, and re-layouts: 9.28 us -> 9.79 us
  transfers between devices with their start and end apart: 3 -> 1, of which waited for: 3 -> 1; matrix products, arithmetic and copies ran while one was open for 1% -> 1% of each run, Pallas kernels for 0% -> 0%
where the time goes in v2:
time: 281 us; the launch traced here: 279 us
  Pallas kernels  99.7 us (35%)
  blocking collectives  52 us (19%)
  waiting for transfers between devices  46.9 us (17%)
  matrix products  41.6 us (15%)
  local copies, waits for them, and re-layouts  22.2 us (8%)
  other arithmetic  12.4 us (4%)
  starting transfers between devices  4.48 us (2%)
    pallas_call x1, Pallas kernels, gather_all(): pl.pallas_call(functools.partial(gather_kernel, count, wide), out_shape=o...  53.5 us
    all_to_all x1, blocking collectives, local(): lax.all_to_all(outgoing, 'sp', split_axis=0, concat_axis=0, tiled=True)  52 us
    all_to_all x1, waiting for transfers between devices, local(): lax.all_to_all(result.reshape(seq_size, item_count, model_width), 'sp', s...  46.9 us
    pallas_call x3, Pallas kernels, swap_tp(): pl.pallas_call(functools.partial(swap_kernel, count, parts.shape[0] == co...  46.2 us
    dot_general x1, matrix products, local(): jnp.einsum('hqk,khv->hqv', weights, valued, preferred_element_type=jnp.fl...  9.83 us
    unnamed x42, local copies, waits for them, and re-layouts  9.79 us
    sub x1, matrix products, probs(): fresh = jnp.exp(masked - jnp.max(masked, axis=-1, keepdims=True))  7.98 us
    dot_general x1, matrix products, local(): jnp.dot(hidden, expert_down[0], preferred_element_type=jnp.float32)  5.96 us
  transfers between devices with their start and end apart: 1, of which 1 were waited for; matrix products, arithmetic and copies ran while one was open for 1% of the time, Pallas kernels for 0%

profile of v2, /device:TPU:0, one launch (start us, length us, event | category | flops | bytes accessed | tf_op | source)
XLA Modules:
  0.0 279.4 jit_solution(5342935172446547216)
XLA Ops:
  7.7 53.5 %gather_keys.1 = (bf16[8,256,256]{2,1,0:T(8,128)(2,1)S(1)}, bf16[8,256,256]{2,1,0:T(8,128)(2,1)S(1)}, bf16[8,256,512]{2,1,0:T(8,128)(2,1)S(1)}, s32[8,1,256]{2,1,0:T(1,128)S(1)}) custom-call(bf16[256,256]{1,0:T(8,128)(2,1)S(1)} %copy-done.4, bf16[256,256]{1,0:T(8,128)(2,1)S(1)} %copy-done.5, bf16[256,512]{1,0:T(8,128)(2,1)S(1)} %copy-done.3, ...), custom_call_target="tpu_custom_call" | custom-call | bytes 3670016 | tf_op jit(solution)/shard_map/gather_keys/pallas_call | solution.py:152
  63.6 2.7 copy.36
  66.2 2.3 reshape.176
  68.6 1.8 copy.38
  70.4 1.6 reshape.178
  71.9 4.0 %reshape.180 = bf16[2048,4,128]{2,1,0:T(4,128)(2,1)} reshape(bf16[8,256,512]{2,1,0:T(8,128)(2,1)} %copy-done.1) | data formatting | bytes 4194304 | tf_op jit(solution)/shard_map/reshape | solution.py:275
  75.9 2.0 fusion.20
  77.9 8.0 %fusion.64 = (f32[4,256]{1,0:T(4,128)}, f32[4,256,2048]{1,2,0:T(8,128)}) fusion(pred[256,2048]{0,1:T(8,128)(4,1)} %fusion.20, bf16[2048,4,64]{0,2,1:T(8,128)(2,1)} %reshape.176, bf16[256,4,64]{0,2,1:T(8,128)(2,1)S(1)} %bitcast.113), kind=kOutput, calls=%fused_computation.87 | convolution fusion | flops 276826112 | bytes 10096640 | tf_op jit(solution)/shard_map/sub | solution.py:269
  85.9 9.8 %multiply_reduce_fusion.1 = (f32[4,256]{1,0:T(4,128)S(1)}, f32[4,256,128]{1,2,0:T(8,128)}) fusion(f32[4,256,2048]{1,2,0:T(8,128)} %get-tuple-element.14, f32[4]{0:T(128)S(1)} %copy-done.19, f32[4,256]{1,0:T(4,128)} %get-tuple-element.13, bf16[2048,4,128]{2,1,0:T(4,128)(2,1)} %reshape.180, pred[256,2048]{0,1:T(8,128)(4,1)} %fusion.20, ...), kind=kOutput, calls=%fused_computation.55 | convolution fusion | flops 822350848 | bytes 12722192 | tf_op jit(solution)/shard_map/hqk,khv->hqv/dot_general | solution.py:276
  96.9 3.3 %convolution_convert_fusion.2 = bf16[256,2048]{1,0:T(8,128)(2,1)} fusion(bf16[256,512]{0,1:T(8,128)(2,1)S(1)} %bitcast.110, bf16[512,2048]{1,0:T(8,128)(2,1)} %param.28), kind=kOutput, calls=%fused_computation.23 | convolution fusion | flops 537395200 | bytes 3407872 | tf_op jit(solution)/shard_map/dot_general | solution.py:283
  100.2 15.6 %swap_tp_1.1 = bf16[4,64,2048]{2,1,0:T(8,128)(2,1)} custom-call(bf16[4,64,2048]{2,1,0:T(8,128)(2,1)} %bitcast.105), custom_call_target="tpu_custom_call" | custom-call | tf_op jit(solution)/shard_map/swap_tp_1/pallas_call | solution.py:208
  118.6 1.8 fusion.40.src
  120.4 15.7 %swap_tp_2.1 = bf16[4,64,2048]{2,1,0:T(8,128)(2,1)} custom-call(bf16[1,64,2048]{2,1,0:T(8,128)(2,1)} %fusion.40.src), custom_call_target="tpu_custom_call" | custom-call | tf_op jit(solution)/shard_map/swap_tp_2/pallas_call | solution.py:208
  136.0 1.9 convolution_convert_fusion
  138.0 52.0 %all_to_all.10 = bf16[8,64,2048]{2,1,0:T(8,128)(2,1)S(1)} all-to-all(bf16[8,64,2048]{2,1,0:T(8,128)(2,1)S(1)} %bitcast.104), channel_id=1, replica_groups=mesh['sp'=8,'tp'=4] {'sp'}, dimensions={0} | all-to-all | bytes 4194304 | tf_op jit(solution)/shard_map/all_to_all | solution.py:311
  192.6 6.0 %convolution_convert_fusion.1 = bf16[512,2048]{1,0:T(8,128)(2,1)} fusion(bf16[1,512,2048]{2,1,0:T(8,128)(2,1)S(1)} %copy-done, bf16[512,2048]{1,0:T(8,128)(2,1)} %bitcast.109, bf16[1,2048,512]{2,1,0:T(8,128)(2,1)} %param.33, f32[512,512]{1,0:T(8,128)S(1)} %fusion.17), kind=kOutput, calls=%fused_computation.18 | convolution fusion | flops 2150105088 | bytes 9437184 | tf_op jit(solution)/shard_map/dot_general | solution.py:317
  198.6 4.5 %all-to-all-start.1 = ((bf16[8,64,2048]{2,1,0:T(8,128)(2,1)}), bf16[8,64,2048]{2,1,0:T(8,128)(2,1)}, u32[]{:S(2)}, u32[]{:S(2)}) async-start(bf16[8,64,2048]{2,1,0:T(8,128)(2,1)} %bitcast.107), calls=%async_computation.1 | async-start | bytes 4194304 | tf_op jit(solution)/shard_map/all_to_all | solution.py:320
  203.2 1.5 fusion.69
  204.7 46.9 %all-to-all-done.1 = bf16[8,64,2048]{2,1,0:T(8,128)(2,1)} async-done(((bf16[8,64,2048]{2,1,0:T(8,128)(2,1)}), bf16[8,64,2048]{2,1,0:T(8,128)(2,1)}, u32[]{:S(2)}, u32[]{:S(2)}) %all-to-all-start.1) | async-done | bytes 2097184 | tf_op jit(solution)/shard_map/all_to_all | solution.py:320
  251.6 2.3 convolution_bitcast_fusion
  253.9 3.6 %fusion.12 = f32[256,2048]{1,0:T(8,128)} fusion(f32[256,2048]{1,0:T(8,128)S(1)} %convolution_bitcast_fusion, bf16[8,64,2048]{2,1,0:T(8,128)(2,1)} %all-to-all-done.1, f32[256,8]{0,1:T(8,128)S(1)} %fusion.54, s32[256,8]{0,1:T(8,128)S(1)} %copy-done.13), kind=kOutput, calls=%fused_computation.22 | convolution fusion | flops 537919488 | bytes 6307840 | tf_op jit(solution)/shard_map/dot_general | solution.py:328
  257.6 3.7 %fusion.13 = bf16[256,2048]{1,0:T(8,128)(2,1)} fusion(f32[256,2048]{1,0:T(8,128)} %fusion.12, bf16[128,2048]{1,0:T(8,128)(2,1)} %param.37, bf16[256,2048]{1,0:T(8,128)(2,1)S(1)} %bitcast.103, bf16[2048,128]{1,0:T(8,128)(2,1)} %param.36, f32[256,128]{1,0:T(8,128)S(1)} %fusion.69), kind=kOutput, calls=%fused_computation.24 | convolution fusion | flops 269680640 | bytes 5373952 | tf_op jit(solution)/shard_map/dot_general | solution.py:335
  261.3 14.9 %swap_tp_3.1 = bf16[4,64,2048]{2,1,0:T(8,128)(2,1)} custom-call(bf16[4,64,2048]{2,1,0:T(8,128)(2,1)} %bitcast.106), custom_call_target="tpu_custom_call" | custom-call | tf_op jit(solution)/shard_map/swap_tp_3/pallas_call | solution.py:208
  277.7 1.7 add_convert_fusion
  (55 shorter events, 18.1 us)
Async XLA Ops:
  0.0 192.6 %copy-start = (bf16[1,512,2048]{2,1,0:T(8,128)(2,1)S(1)}, bf16[1,512,2048]{2,1,0:T(8,128)(2,1)}, u32[]{:S(2)}) copy-start(bf16[1,512,2048]{2,1,0:T(8,128)(2,1)} %param.34) | copy-start | bytes 6291460
  1.6 0.6 copy-start.12
  4.3 1.0 copy-start.3
  5.2 0.9 copy-start.4
  6.1 0.9 copy-start.5
  7.0 0.7 copy-start.6
  61.2 1.4 copy-start.1
  62.6 1.0 copy-start.2
  71.9 4.0 %copy-start.7 = (s32[256]{0:T(256)S(1)}, s32[256]{0:T(256)}, u32[]{:S(2)}) copy-start(s32[256]{0:T(256)} %param.25) | copy-start | bytes 3076
  77.9 8.0 %copy-start.19 = (f32[4]{0:T(128)S(1)}, f32[4]{0:T(128)}, u32[]{:S(2)}) copy-start(f32[4]{0:T(128)} %param.26) | copy-start | bytes 52
  85.9 9.8 %copy-start.17 = (f32[128]{0:T(128)S(1)}, f32[128]{0:T(128)}, u32[]{:S(2)}) copy-start(f32[128]{0:T(128)} %param.27) | copy-start | bytes 1540
  100.2 18.4 %copy-start.15 = (f32[2048]{0:T(1024)S(1)}, f32[2048]{0:T(1024)}, u32[]{:S(2)}) copy-start(f32[2048]{0:T(1024)} %param.29) | copy-start | bytes 24580
  117.3 20.7 %copy-start.9 = (f32[64,2048]{1,0:T(8,128)}, f32[64,2048]{1,0:T(8,128)S(1)}, u32[]{:S(2)}) copy-start(f32[64,2048]{1,0:T(8,128)S(1)} %convert_reduce_fusion.1) | copy-start | bytes 1572868
  138.0 53.4 %copy-start.18 = (bf16[1,2048,512]{2,1,0:T(8,128)(2,1)S(1)}, bf16[1,2048,512]{2,1,0:T(8,128)(2,1)}, u32[]{:S(2)}) copy-start(bf16[1,2048,512]{2,1,0:T(8,128)(2,1)} %param.32) | copy-start | bytes 6291460
  190.0 1.4 copy-start.11
  198.6 4.5 %copy-start.14 = (s32[256,4]{0,1:T(4,128)S(1)}, s32[256,4]{0,1:T(4,128)}, u32[]{:S(2)}) copy-start(s32[256,4]{0,1:T(4,128)} %param.30) | copy-start | bytes 12292
  198.6 4.5 %copy-start.16 = (f32[256,4]{0,1:T(4,128)S(1)}, f32[256,4]{0,1:T(4,128)}, u32[]{:S(2)}) copy-start(f32[256,4]{0,1:T(4,128)} %param.31) | copy-start | bytes 12292
  198.6 4.6 %copy-start.8 = (bf16[4,64,2048]{2,1,0:T(8,128)(2,1)S(1)}, bf16[4,64,2048]{2,1,0:T(8,128)(2,1)}, u32[]{:S(2)}) copy-start(bf16[4,64,2048]{2,1,0:T(8,128)(2,1)} %swap_tp_2.1) | copy-start | bytes 3145732
  198.6 53.0 %copy-start.13 = (s32[256,8]{0,1:T(8,128)S(1)}, s32[256,8]{0,1:T(8,128)}, u32[]{:S(2)}) copy-start(s32[256,8]{0,1:T(8,128)} %copy-done.12) | copy-start | bytes 24580
  198.6 53.0 %all-to-all-start.1 = ((bf16[8,64,2048]{2,1,0:T(8,128)(2,1)}), bf16[8,64,2048]{2,1,0:T(8,128)(2,1)}, u32[]{:S(2)}, u32[]{:S(2)}) async-start(bf16[8,64,2048]{2,1,0:T(8,128)(2,1)} %bitcast.107), calls=%async_computation.1 | async-start | bytes 4194304 | tf_op jit(solution)/shard_map/all_to_all | solution.py:320
  261.3 16.4 %copy-start.10 = (f32[64,2048]{1,0:T(8,128)S(1)}, f32[64,2048]{1,0:T(8,128)}, u32[]{:S(2)}) copy-start(f32[64,2048]{1,0:T(8,128)} %copy-done.9) | copy-start | bytes 1572868
